TPU v7x, 256 devices: a 4x2x16 block of a 4x16x16 slice. The times are simulated.
256 devices in a mesh: grp: 2 (over y), ep: 32 (over z, core), tp: 4 (over x).
Axes of the slice: x: 4, y: 2, z: 16, core: 2. Of those that a mesh axis runs over, the one named last changes fastest.
The devices are a block of a 4x16x16 slice.
Arguments:
- queries: bfloat16 [24576, 1024], P(('grp', 'ep'), 'tp'), parts along dimension 0, may hold values from -6 to 6
- key_values: bfloat16 [24576, 512], P(('grp', 'ep'), 'tp'), parts along dimension 0, may hold values from -6 to 6
- query_gain: float32 [64], replicated, may hold values from 0.5 to 5
- key_gain: float32 [64], replicated, may hold values from 0.5 to 5
- out_weight: bfloat16 [1024, 2048], P('tp'), may hold values from -0.1875 to 0.1875
- second_batch: bfloat16 [32768, 2048], P(('grp', 'ep', 'tp')), parts along dimension 0, may hold values from -6 to 6
- norm_gain: float32 [2048], replicated, may hold values from 0.1 to 1.9
- routes: int32 [32768, 2], P(('grp', 'ep', 'tp')), parts along dimension 0, may hold values from 0 to 63, all different within a row; in each aligned block of 128 rows (0 to 127, 128 to 255, ...) at most 6 rows name the same one
- route_weights: float32 [32768, 2], P(('grp', 'ep', 'tp')), parts along dimension 0, may hold values from 0.2 to 1
- expert_gate: bfloat16 [64, 2048, 1024], P('ep', None, 'tp'), may hold values from -0.125 to 0.125
- expert_up: bfloat16 [64, 2048, 1024], P('ep', None, 'tp'), may hold values from -0.125 to 0.125
- expert_down: bfloat16 [64, 1024, 2048], P('ep', 'tp'), may hold values from -0.1875 to 0.1875
- shared_gate: bfloat16 [2048, 512], P(None, 'tp'), may hold values from -0.125 to 0.125
- shared_up: bfloat16 [2048, 512], P(None, 'tp'), may hold values from -0.125 to 0.125
- shared_down: bfloat16 [512, 2048], P('tp'), may hold values from -0.25 to 0.25
Outputs:
- mixer_out: bfloat16 [24576, 2048], P(('grp', 'ep', 'tp')), parts along dimension 0
- channel_out: bfloat16 [32768, 2048], P(('grp', 'ep', 'tp')), parts along dimension 0
There are 2 independent parts, one for each index of `grp`. A program takes and returns all parts, laid end to end along the dimension named above; an argument that names none is the same for every part. Nothing has to cross between parts.
Inputs may be any that keep to these rules, and one draw needn't show every extreme that they name: `routes`: each row names 2 different experts. Among the rows of one device no expert is named more than 6 times, and in every draw some expert is named exactly 6 times by the rows of some device.
All inputs are finite; a program needn't handle non-finite values.
Results may differ from a plain program's by a relative error of at most 0.015.
The roundings to bfloat16 on the way count: a program that leaves them out, or rounds other values in their place, can miss the bound.
Values may be sent and summed in bfloat16 or wider, within the bound.
A program may use at most 128 MiB of HBM per device.

v0:
```python
import jax
import jax.numpy as jnp
from jax import lax
from jax.sharding import Mesh
from jax.sharding import PartitionSpec as P

GRID_W = 64
EP = ("ep_0", "ep_1")
GRP_EP = ("grp", "ep_0", "ep_1")
GRP_EP_TP = ("grp", "ep_0", "ep_1", "tp")
rope_base = 10000.0
norm_eps = 1e-06


def joined_along(tiles, dim):
    shape = list(tiles.shape[1:])
    shape[dim] *= tiles.shape[0]
    return jnp.moveaxis(tiles, 0, dim).reshape(shape)


def stacked_from(shard, axes, order):
    tiles = shard
    for k in order:
        tiles = lax.all_gather(tiles, axes[k])
    done = order[::-1]
    back = [done.index(k) for k in range(len(axes))]
    tiles = tiles.transpose(*back, *range(len(axes), tiles.ndim))
    return tiles.reshape(-1, *shard.shape)


def whole_of(shard, axes, order, dim):
    return joined_along(stacked_from(shard, axes, order), dim)


def from_everyone(shard, axis):
    copies = jnp.broadcast_to(shard, (lax.axis_size(axis), *shard.shape))
    return lax.all_to_all(copies, axis, split_axis=0, concat_axis=0, tiled=True)


def gathered_copies(shard, axis, dim):
    return joined_along(from_everyone(shard, axis), dim)


def in_blocks(shard, dim, length):
    shape = shard.shape
    tiles = shard.reshape(*shape[:dim], length, shape[dim] // length, *shape[dim + 1 :])
    return jnp.moveaxis(tiles, dim, 0)


def summed_on_arrival(shard, axis, dim):
    tiles = in_blocks(shard, dim, lax.axis_size(axis))
    arrived = lax.all_to_all(tiles, axis, split_axis=0, concat_axis=0, tiled=True)
    return arrived.astype(jnp.float32).sum(axis=0)


def head_norm(vectors, gain):
    return (
        vectors * lax.rsqrt(jnp.mean(vectors * vectors, axis=-1, keepdims=True) + norm_eps) * gain
    )


def turn_heads(vectors, positions):
    row_count, head_count, head_size = vectors.shape
    half_size = head_size // 2
    inverse = rope_base ** (-jnp.arange(0, half_size, 2, dtype=jnp.float32) / half_size)
    grid_row = (positions // GRID_W).astype(jnp.float32)
    grid_column = (positions % GRID_W).astype(jnp.float32)
    angles = jnp.concatenate([grid_row[:, None] * inverse, grid_column[:, None] * inverse], axis=-1)
    cosine = jnp.cos(angles)[:, None, :]
    sine = jnp.sin(angles)[:, None, :]
    paired = vectors.reshape(row_count, head_count, half_size, 2)
    first = paired[..., 0]
    second = paired[..., 1]
    turned = jnp.stack([first * cosine - second * sine, first * sine + second * cosine], axis=-1)
    return turned.reshape(vectors.shape)


def slot_ids(route_rows, expert_count, capacity):
    row_count, top_count = route_rows.shape
    flat_routes = route_rows.reshape(-1)
    onehot = (flat_routes[:, None] == jnp.arange(expert_count, dtype=jnp.int32)[None, :]).astype(
        jnp.int32
    )
    earlier = jnp.cumsum(onehot, axis=0) - onehot
    within = jnp.sum(earlier * onehot, axis=1)
    return (flat_routes * capacity + within).reshape(row_count, top_count)


def slot_table(slots, slot_count):
    row_count, top_count = slots.shape
    flat_slots = slots.reshape(-1)
    owner_row = jnp.arange(row_count * top_count, dtype=jnp.int32) // top_count
    matches = flat_slots[None, :] == jnp.arange(slot_count, dtype=jnp.int32)[:, None]
    occupied = jnp.any(matches, axis=1)
    source_row = jnp.sum(jnp.where(matches, owner_row[None, :], 0), axis=1)
    return jnp.where(occupied, source_row, row_count)


def pick_block(row_count):
    for candidate in range(min(row_count, 1024), 0, -1):
        if row_count % candidate == 0:
            return candidate
    return row_count


def attend_keys(query_turned, scale, running, pieces):
    head_size = query_turned.shape[-1]
    key_block = pick_block(pieces.shape[0])
    blocks = pieces.reshape(pieces.shape[0] // key_block, key_block, 2 * head_size)

    def one_block(carried, block_rows):
        top_now, total_now, acc_now = carried
        scores = (
            jnp.einsum(
                "qhd,kd->hqk",
                query_turned,
                block_rows[:, :head_size],
                preferred_element_type=jnp.float32,
            )
            * scale
        )
        top_new = jnp.maximum(top_now, jnp.max(scores, axis=-1))
        shrink = jnp.exp(top_now - top_new)
        exps = jnp.exp(scores - top_new[..., None])
        total_new = total_now * shrink + jnp.sum(exps, axis=-1)
        acc_new = acc_now * shrink[..., None] + jnp.einsum(
            "hqk,kd->hqd",
            exps.astype(jnp.bfloat16),
            block_rows[:, head_size:],
            preferred_element_type=jnp.float32,
        )
        return ((top_new, total_new, acc_new), None)

    result, ignored = lax.scan(one_block, running, blocks)
    return result


def shared_hidden_of(token_rows, gate_weights, up_weights):
    gate_part = jnp.dot(token_rows, gate_weights, preferred_element_type=jnp.float32)
    up_part = jnp.dot(token_rows, up_weights, preferred_element_type=jnp.float32)
    return (jax.nn.silu(gate_part) * up_part).astype(jnp.bfloat16)


def expert_hidden(slot_rows, gate_weights, up_weights):
    gate_part = jnp.einsum(
        "osjcd,jdf->osjcf", slot_rows, gate_weights, preferred_element_type=jnp.float32
    )
    up_part = jnp.einsum(
        "osjcd,jdf->osjcf", slot_rows, up_weights, preferred_element_type=jnp.float32
    )
    return (jax.nn.silu(gate_part) * up_part).astype(jnp.bfloat16)


def body(
    queries,
    key_values,
    query_gain,
    key_gain,
    out_weight,
    second_batch,
    norm_gain,
    routes,
    route_weights,
    expert_gate,
    expert_up,
    expert_down,
    shared_gate,
    shared_up,
    shared_down,
):
    query_rows = queries.shape[0]
    head_size = query_gain.shape[0]
    heads_here = queries.shape[1] // head_size
    ep_count = lax.axis_size(EP)
    positions = lax.axis_index(EP) * query_rows + jnp.arange(query_rows, dtype=jnp.int32)
    query_turned = turn_heads(
        head_norm(
            queries.reshape(query_rows, heads_here, head_size).astype(jnp.float32), query_gain
        ),
        positions,
    ).astype(jnp.bfloat16)
    key_turned = turn_heads(
        head_norm(key_values[:, None, :head_size].astype(jnp.float32), key_gain), positions
    ).astype(jnp.bfloat16)
    keys_and_values = jnp.concatenate([key_turned[:, 0, :], key_values[:, head_size:]], axis=1)
    start_state = (
        jnp.full((heads_here, query_rows), -1e30, jnp.float32),
        jnp.zeros((heads_here, query_rows), jnp.float32),
        jnp.zeros((heads_here, query_rows, head_size), jnp.float32),
    )
    top_all, total_all, acc_all = attend_keys(
        query_turned, head_size ** (-0.5), start_state, whole_of(keys_and_values, EP, (0, 1), 0)
    )
    head_out = (
        (acc_all / total_all[..., None])
        .transpose(1, 0, 2)
        .reshape(query_rows, heads_here * head_size)
        .astype(jnp.bfloat16)
    )
    tok_count = second_batch.shape[0]
    model_width = second_batch.shape[1]
    top_count = routes.shape[1]
    local_experts = expert_gate.shape[0]
    expert_count = local_experts * ep_count
    capacity = 3 * tok_count * top_count // (2 * expert_count)
    slot_count = expert_count * capacity
    token_float = second_batch.astype(jnp.float32)
    normed = (
        token_float
        * lax.rsqrt(jnp.mean(token_float * token_float, axis=-1, keepdims=True) + norm_eps)
        * norm_gain
    ).astype(jnp.bfloat16)
    own_slots = slot_ids(routes, expert_count, capacity)
    shared_hidden = (lambda pieces, begin_at: shared_hidden_of(pieces, shared_gate, shared_up))(
        gathered_copies(normed, "tp", 0), jnp.int32(0)
    )
    outgoing = jnp.take(
        normed, slot_table(own_slots, slot_count), axis=0, mode="fill", fill_value=0
    )[None]
    arrived = lax.all_to_all(outgoing, EP, split_axis=1, concat_axis=1, tiled=True)
    arrived = arrived.reshape(arrived.shape[0], ep_count, local_experts, capacity, model_width)
    hidden = expert_hidden(
        lax.all_gather(arrived, "tp", axis=0, tiled=True), expert_gate, expert_up
    )
    routed_part = jnp.einsum(
        "osjcf,jfd->osjcd", hidden, expert_down, preferred_element_type=jnp.float32
    ).reshape(-1, model_width)
    shared_part = jnp.dot(shared_hidden, shared_down, preferred_element_type=jnp.float32)
    head_partial = jnp.dot(head_out, out_weight, preferred_element_type=jnp.float32)
    attn_sum, routed_sum, shared_sum = (
        summed_on_arrival(head_partial.astype(jnp.bfloat16), "tp", 0),
        summed_on_arrival(routed_part.astype(jnp.bfloat16), "tp", 0),
        summed_on_arrival(shared_part.astype(jnp.bfloat16), "tp", 0),
    )
    returned = lax.all_to_all(
        routed_sum.astype(jnp.bfloat16), EP, split_axis=0, concat_axis=0, tiled=True
    )
    combined = shared_sum
    for slot_pick in range(top_count):
        combined = combined + route_weights[:, slot_pick : slot_pick + 1] * jnp.take(
            returned, own_slots[:, slot_pick], axis=0
        ).astype(jnp.float32)
    return (attn_sum.astype(jnp.bfloat16), combined.astype(jnp.bfloat16))


def solution(mesh):
    torus = Mesh(
        mesh.devices.reshape(mesh.shape["grp"], 16, 2, mesh.shape["tp"]),
        ("grp", "ep_0", "ep_1", "tp"),
    )
    return jax.shard_map(
        body,
        mesh=torus,
        in_specs=(
            P(GRP_EP, "tp"),
            P(GRP_EP, "tp"),
            P(),
            P(),
            P("tp", None),
            P(GRP_EP_TP, None),
            P(),
            P(GRP_EP_TP, None),
            P(GRP_EP_TP, None),
            P(EP, None, "tp"),
            P(EP, None, "tp"),
            P(EP, "tp", None),
            P(None, "tp"),
            P(None, "tp"),
            P("tp", None),
        ),
        out_specs=(P(GRP_EP_TP, None), P(GRP_EP_TP, None)),
        check_vma=False,
    )
```

profile of v0, /device:TPU:33, one launch (start us, length us, event | category | flops | bytes accessed | tf_op | source)
XLA Modules:
  0.0 621.9 jit_solution(13244901644372939689)
XLA Ops:
  17.1 4.1 copy.120
  21.7 12.4 %reduce.10 = bf16[384,2048]{1,0:T(8,128)(2,1)} reduce(bf16[384,1,2048]{2,1,0:T(2,128)(2,1)} %bitcast.152, bf16[]{:T(256)} %broadcast.416), dimensions={1}, to_apply=%bitcast.134.reduce_sub_computation | reduce | bytes 3145730
  34.1 5.2 reshape.492
  39.3 25.6 %all-to-all-start.3 = ((bf16[32,2,12288]{2,1,0:T(2,128)(2,1)}), bf16[32,2,12288]{2,1,0:T(2,128)(2,1)}, u32[]{:S(2)}, u32[]{:S(2)}) async-start(bf16[32,2,12288]{2,1,0:T(2,128)(2,1)} %reshape.492), calls=%async_computation.3 | async-start | bytes 3145728 | tf_op jit(solution)/shard_map/all_to_all | solution.py:220
  66.8 95.3 %all-gather.8.cloned.1.call-done = bf16[6144,128]{0,1:T(8,128)(2,1)} async-done(((bf16[384,128]{0,1:T(8,128)(2,1)}), bf16[6144,128]{0,1:T(8,128)(2,1)}) %all-gather.8.cloned.1.call-update) | async-done | bytes 1572880 | tf_op jit(solution)/shard_map/all_gather | solution.py:24
  164.9 9.5 %reshape.493 = bf16[384,1,2048]{2,1,0:T(2,128)(2,1)} reshape(bf16[32,2,12288]{2,1,0:T(2,128)(2,1)} %all-to-all-done.3) | data formatting | bytes 3145728
  174.3 12.2 %bitcast_reduce_fusion.2 = bf16[384,2048]{1,0:T(8,128)(2,1)} fusion(bf16[384,1,2048]{2,1,0:T(2,128)(2,1)} %reshape.493), kind=kLoop, calls=%fused_computation.129 | loop fusion | bytes 3145728 | tf_op jit(solution)/shard_map/all_to_all | solution.py:220
  195.7 4.8 all-to-all-start.1
  202.6 25.4 %all-to-all-done.1 = bf16[4,128,2048]{2,1,0:T(8,128)(2,1)} async-done(((bf16[4,128,2048]{2,1,0:T(8,128)(2,1)}), bf16[4,128,2048]{2,1,0:T(8,128)(2,1)}, u32[]{:S(2)}, u32[]{:S(2)}) %all-to-all-start.1) | async-done | bytes 2097184 | tf_op jit(solution)/shard_map/all_to_all | solution.py:37
  230.3 5.5 convolution_convert_fusion
  235.8 4.5 all-to-all-start.2
  244.4 55.9 %all-gather.6.cloned.1.call-done = bf16[4,32,2,6,2048]{4,1,3,0,2:T(8,128)(2,1)} async-done(((bf16[1,32,2,6,2048]{4,1,3,0,2:T(8,128)(2,1)}), bf16[4,32,2,6,2048]{4,1,3,0,2:T(8,128)(2,1)}) %all-gather.6.cloned.1.call-update) | async-done | bytes 6291472 | tf_op jit(solution)/shard_map/all_gather | solution.py:223
  300.3 6.4 %fusion.14 = f32[2,4,32,6,256]{4,2,3,1,0:T(8,128)} fusion(bf16[4,32,2,6,2048]{4,1,3,0,2:T(8,128)(2,1)} %all-gather.6.cloned.1.call-done, bf16[2,2048,256]{2,1,0:T(8,128)(2,1)} %param.28), kind=kOutput, calls=%fused_computation.27 | convolution fusion | flops 1610612736 | bytes 9961472 | tf_op jit(solution)/shard_map/osjcd,jdf->osjcf/dot_general | solution.py:145
  306.7 10.1 %convert_bitcast_fusion = bf16[4,32,2,6,2048]{4,1,3,0,2:T(8,128)(2,1)} fusion(bf16[2,256,2048]{2,1,0:T(8,128)(2,1)S(1)} %copy-done, f32[2,4,32,6,256]{4,2,3,1,0:T(8,128)} %fusion.14, bf16[4,32,2,6,2048]{4,1,3,0,2:T(8,128)(2,1)} %all-gather.6.cloned.1.call-done, bf16[2,2048,256]{2,1,0:T(8,128)(2,1)} %param.29), kind=kOutput, calls=%fused_computation.20 | convolution fusion | flops 3226730496 | bytes 18350080 | tf_op jit(solution)/shard_map/osjcf,jfd->osjcd/dot_general | solution.py:225
  316.8 10.2 %copy.100 = bf16[4,32,2,6,2048]{4,0,3,2,1:T(4,128)(2,1)} copy(bf16[4,32,2,6,2048]{4,1,3,0,2:T(8,128)(2,1)} %convert_bitcast_fusion) | data formatting | bytes 12582912 | tf_op jit(solution)/shard_map/convert_element_type | solution.py:232
  327.0 9.1 %copy.101 = bf16[4,384,2048]{2,1,0:T(8,128)(2,1)} copy(bf16[4,384,2048]{2,0,1:T(4,128)(2,1)} %bitcast.151) | data formatting | bytes 12582912 | tf_op jit(solution)/shard_map/convert_element_type | solution.py:232
  336.1 5.3 all-to-all-start.4
  341.5 127.8 %while.15 = (s32[]{:T(128)}, f32[4,384]{1,0:T(4,128)S(1)}, f32[4,384]{1,0:T(4,128)S(1)}, f32[4,384,64]{1,2,0:T(8,128)S(1)}, bf16[12,1024,128]{2,1,0:T(8,128)(2,1...) while((s32[]{:T(128)}, f32[4,384]{1,0:T(4,128)S(1)}, f32[4,384]{1,0:T(4,128)S(1)}, ...), condition=%wide.region_5.6_spmd.clone, body=%wide.region_2.5_spmd.clone.sunk | while | flops 415538688 | bytes 46432384 | solution.py:134
  471.1 4.1 all-to-all-start
  475.3 5.7 reduce_sum.96
  484.5 10.4 %all-to-all-done = bf16[4,96,2048]{2,1,0:T(8,128)(2,1)S(1)} async-done(((bf16[4,96,2048]{2,1,0:T(8,128)(2,1)}), bf16[4,96,2048]{2,1,0:T(8,128)(2,1)S(1)}, u32[]{:S(2)}, u32[]{:S(2)}) %all-to-all-start) | async-done | bytes 1572896 | tf_op jit(solution)/shard_map/all_to_all | solution.py:52
  495.0 11.2 %all-to-all-start.5 = ((bf16[32,12,2048]{2,1,0:T(8,128)(2,1)}), bf16[32,12,2048]{2,1,0:T(8,128)(2,1)}, u32[]{:S(2)}, u32[]{:S(2)}) async-start(bf16[32,12,2048]{2,1,0:T(8,128)(2,1)} %all_to_all.28), calls=%async_computation.5 | async-start | bytes 4194304 | tf_op jit(solution)/shard_map/all_to_all | solution.py:235
  509.6 94.8 %all-to-all-done.5 = bf16[32,12,2048]{2,1,0:T(8,128)(2,1)} async-done(((bf16[32,12,2048]{2,1,0:T(8,128)(2,1)}), bf16[32,12,2048]{2,1,0:T(8,128)(2,1)}, u32[]{:S(2)}, u32[]{:S(2)}) %all-to-all-start.5) | async-done | bytes 1572896 | tf_op jit(solution)/shard_map/all_to_all | solution.py:235
  608.7 4.0 gather_fusion.2
  (220 shorter events, 175.0 us)
Async XLA Ops:
  7.2 299.5 %copy-start = (bf16[2,256,2048]{2,1,0:T(8,128)(2,1)S(1)}, bf16[2,256,2048]{2,1,0:T(8,128)(2,1)}, u32[]{:S(2)}) copy-start(bf16[2,256,2048]{2,1,0:T(8,128)(2,1)} %param.30) | copy-start | bytes 6291460
  39.3 25.7 %copy-start.5 = (bf16[384,128]{1,0:T(8,128)(2,1)S(1)}, bf16[384,128]{1,0:T(8,128)(2,1)}, u32[]{:S(2)}) copy-start(bf16[384,128]{1,0:T(8,128)(2,1)} %param.20) | copy-start | bytes 294916
  39.3 26.0 %copy-start.9 = (f32[64]{0:T(128)S(1)}, f32[64]{0:T(128)}, u32[]{:S(2)}) copy-start(f32[64]{0:T(128)} %param.22) | copy-start | bytes 772
  39.3 125.6 %all-to-all-start.3 = ((bf16[32,2,12288]{2,1,0:T(2,128)(2,1)}), bf16[32,2,12288]{2,1,0:T(2,128)(2,1)}, u32[]{:S(2)}, u32[]{:S(2)}) async-start(bf16[32,2,12288]{2,1,0:T(2,128)(2,1)} %reshape.492), calls=%async_computation.3 | async-start | bytes 3145728 | tf_op jit(solution)/shard_map/all_to_all | solution.py:220
  64.9 97.2 %all-gather.8.cloned.1.call-start = ((), (), s32[]{:S(2)}) async-start(), calls=%async_computation.7 | async-start | bytes 1671168 | tf_op jit(solution)/shard_map/all_gather | solution.py:24
  66.7 173.7 %all-gather.10.cloned.1.call-start = ((), (), s32[]{:S(2)}) async-start(), calls=%async_computation.8 | async-start | bytes 4718592 | tf_op jit(solution)/shard_map/all_gather | solution.py:24
  164.8 135.5 %all-gather.6.cloned.1.call-start = ((), (), s32[]{:S(2)}) async-start(), calls=%async_computation.6 | async-start | bytes 7864320 | tf_op jit(solution)/shard_map/all_gather | solution.py:223
  195.7 4.9 copy-start.6
  195.7 5.3 copy-start.10
  195.7 32.2 %all-to-all-start.1 = ((bf16[4,128,2048]{2,1,0:T(8,128)(2,1)}), bf16[4,128,2048]{2,1,0:T(8,128)(2,1)}, u32[]{:S(2)}, u32[]{:S(2)}) async-start(bf16[4,128,2048]{2,1,0:T(8,128)(2,1)} %broadcast_in_dim.47), calls=%async_computation.1 | async-start | bytes 4194304 | tf_op jit(solution)/shard_map/all_to_all | solution.py:37
  235.8 100.3 %all-to-all-start.2 = ((bf16[4,128,2048]{2,1,0:T(8,128)(2,1)}), bf16[4,128,2048]{2,1,0:T(8,128)(2,1)}, u32[]{:S(2)}, u32[]{:S(2)}) async-start(bf16[4,128,2048]{2,1,0:T(8,128)(2,1)} %bitcast.153), calls=%async_computation.2 | async-start | bytes 4194304 | tf_op jit(solution)/shard_map/all_to_all | solution.py:52
  336.1 135.0 %all-to-all-start.4 = ((bf16[4,384,2048]{2,1,0:T(8,128)(2,1)}), bf16[4,384,2048]{2,1,0:T(8,128)(2,1)}, u32[]{:S(2)}, u32[]{:S(2)}) async-start(bf16[4,384,2048]{2,1,0:T(8,128)(2,1)} %copy.101), calls=%async_computation.4 | async-start | bytes 12582912 | tf_op jit(solution)/shard_map/all_to_all | solution.py:52
  341.4 127.9 %copy-start.4 = (bf16[256,2048]{1,0:T(8,128)(2,1)S(1)}, bf16[256,2048]{1,0:T(8,128)(2,1)}, u32[]{:S(2)}) copy-start(bf16[256,2048]{1,0:T(8,128)(2,1)} %param.23) | copy-start | bytes 3145732
  346.3 4.6 copy-start.2
  357.0 4.6 copy-start.2
  367.6 4.6 copy-start.2
  388.9 4.6 copy-start.2
  410.2 4.6 copy-start.2
  431.5 4.6 copy-start.2
  471.1 23.9 %all-to-all-start = ((bf16[4,96,2048]{2,1,0:T(8,128)(2,1)}), bf16[4,96,2048]{2,1,0:T(8,128)(2,1)S(1)}, u32[]{:S(2)}, u32[]{:S(2)}) async-start(bf16[4,96,2048]{2,1,0:T(8,128)(2,1)} %bitcast.156), calls=%async_computation | async-start | bytes 3145728 | tf_op jit(solution)/shard_map/all_to_all | solution.py:52
  484.5 21.8 %copy-start.7 = (s32[128,2]{0,1:T(2,128)S(1)}, s32[128,2]{0,1:T(2,128)}, u32[]{:S(2)}) copy-start(s32[128,2]{0,1:T(2,128)} %param.26) | copy-start | bytes 3076
  484.5 21.9 %copy-start.8 = (f32[128,2]{0,1:T(2,128)S(1)}, f32[128,2]{0,1:T(2,128)}, u32[]{:S(2)}) copy-start(f32[128,2]{0,1:T(2,128)} %param.27) | copy-start | bytes 3076
  495.0 109.4 %all-to-all-start.5 = ((bf16[32,12,2048]{2,1,0:T(8,128)(2,1)}), bf16[32,12,2048]{2,1,0:T(8,128)(2,1)}, u32[]{:S(2)}, u32[]{:S(2)}) async-start(bf16[32,12,2048]{2,1,0:T(8,128)(2,1)} %all_to_all.28), calls=%async_computation.5 | async-start | bytes 4194304 | tf_op jit(solution)/shard_map/all_to_all | solution.py:235
  608.7 6.4 %copy-start.1 = (bf16[2,256,2048]{2,1,0:T(8,128)(2,1)S(1)}, bf16[2,256,2048]{2,1,0:T(8,128)(2,1)}, u32[]{:S(2)}) copy-start(bf16[2,256,2048]{2,1,0:T(8,128)(2,1)} %param.30) | copy-start | bytes 6291460
  (7 other events, 29.3 us)
Sparse Core Ops, SparseCore 0:
  68.1 93.9 all-gather.7
  164.9 24.2 all-gather.9
  194.1 106.1 all-gather.5
where the time goes:
time: 626 us; the launch traced here: 622 us
  waiting for transfers between devices  282 us (45%)
  local copies, waits for them, and re-layouts  105 us (17%)
  matrix products  84.7 us (14%)
  other arithmetic  79.3 us (13%)
  starting transfers between devices  55.8 us (9%)
  between operations  14.5 us (2%)
    all_gather x2, waiting for transfers between devices, stacked_from(): tiles = lax.all_gather(tiles, axes[k])  95.4 us
    all_to_all x1, waiting for transfers between devices, body(): lax.all_to_all(routed_sum.astype(jnp.bfloat16), EP, split_axis=0, concat_...  94.8 us
    all_gather x1, waiting for transfers between devices, body(): lax.all_gather(arrived, 'tp', axis=0, tiled=True)  55.9 us
    reduce_sum x12, other arithmetic, one_block(): total_new = total_now * shrink + jnp.sum(exps, axis=-1)  47.6 us
    dot_general x12, matrix products, one_block(): jnp.einsum('qhd,kd->hqk', query_turned, block_rows[:, :head_size], prefer...  43.5 us
    all_to_all x1, starting transfers between devices, body(): lax.all_to_all(outgoing, EP, split_axis=1, concat_axis=1, tiled=True)  25.6 us
    all_to_all x1, waiting for transfers between devices, from_everyone(): return lax.all_to_all(copies, axis, split_axis=0, concat_axis=0, tiled=True)  25.4 us
    convert_element_type x2, local copies, waits for them, and re-layouts, body(): routed_part.astype(jnp.bfloat16)  19.3 us
  transfers between devices with their start and end apart: 9, of which 5 were waited for; matrix products, arithmetic and copies ran while one was open for 35% of the time, Pallas kernels for 0%

commit v1 on v0

--- a/solution.py
+++ b/solution.py
@@ -217,7 +217,9 @@
     outgoing = jnp.take(
         normed, slot_table(own_slots, slot_count), axis=0, mode="fill", fill_value=0
     )[None]
-    arrived = lax.all_to_all(outgoing, EP, split_axis=1, concat_axis=1, tiled=True)
+    parts = jnp.split(outgoing, lax.axis_size(EP), axis=1)
+    got = lax.all_to_all(jnp.stack(parts), EP, 0, 0)
+    arrived = jnp.concatenate(got, axis=1)
     arrived = arrived.reshape(arrived.shape[0], ep_count, local_experts, capacity, model_width)
     hidden = expert_hidden(
         lax.all_gather(arrived, "tp", axis=0, tiled=True), expert_gate, expert_up

time: 626 us -> 598 us (0.955)
  local copies, waits for them, and re-layouts: 105 us -> 90.2 us
  other arithmetic: 79.3 us -> 65.5 us
    all_to_all x1, waiting for transfers between devices: 0.01 us -> 55.8 us  [body(): got = lax.all_to_all(jnp.stack(parts), EP, 0, 0)]
    all_gather x2, waiting for transfers between devices: 95.4 us -> 45.3 us  [stacked_from(): tiles = lax.all_gather(tiles, axes[k])]
    unnamed x4 -> x3, other arithmetic: 12.4 us -> 0.01 us
    all_to_all x1, waiting for transfers between devices: 25.4 us -> 37.5 us  [from_everyone(): return lax.all_to_all(copies, axis, split_axis=0, concat_axis=0, tiled=True)]
    all_gather x1, waiting for transfers between devices: 55.9 us -> 43.9 us  [body(): lax.all_gather(arrived, 'tp', axis=0, tiled=True)]
    all_to_all x1, local copies, waits for them, and re-layouts: 12.2 us -> 3.62 us  [body(): got = lax.all_to_all(jnp.stack(parts), EP, 0, 0)]
    reshape x2 -> x0, local copies, waits for them, and re-layouts: 7.34 us -> none  [body(): arrived.reshape(arrived.shape[0], ep_count, local_experts, capacity, mode...]
    unnamed x27 -> x55, local copies, waits for them, and re-layouts: 16.6 us -> 20.3 us
  transfers between devices with their start and end apart: 9 -> 9, of which waited for: 5 -> 6; matrix products, arithmetic and copies ran while one was open for 35% -> 36% of each run, Pallas kernels for 0% -> 0%
where the time goes in v1:
time: 598 us; the launch traced here: 596 us
  waiting for transfers between devices  288 us (48%)
  local copies, waits for them, and re-layouts  90.2 us (15%)
  matrix products  84.5 us (14%)
  other arithmetic  65.5 us (11%)
  starting transfers between devices  53 us (9%)
  between operations  14.2 us (2%)
    all_to_all x1, waiting for transfers between devices, body(): lax.all_to_all(routed_sum.astype(jnp.bfloat16), EP, split_axis=0, concat_...  95.3 us
    all_to_all x1, waiting for transfers between devices, body(): got = lax.all_to_all(jnp.stack(parts), EP, 0, 0)  55.8 us
    reduce_sum x12, other arithmetic, one_block(): total_new = total_now * shrink + jnp.sum(exps, axis=-1)  47.6 us
    all_gather x2, waiting for transfers between devices, stacked_from(): tiles = lax.all_gather(tiles, axes[k])  45.3 us
    all_gather x1, waiting for transfers between devices, body(): lax.all_gather(arrived, 'tp', axis=0, tiled=True)  43.9 us
    dot_general x12, matrix products, one_block(): jnp.einsum('qhd,kd->hqk', query_turned, block_rows[:, :head_size], prefer...  43.2 us
    all_to_all x1, waiting for transfers between devices, from_everyone(): return lax.all_to_all(copies, axis, split_axis=0, concat_axis=0, tiled=True)  37.5 us
    all_to_all x1, starting transfers between devices, body(): got = lax.all_to_all(jnp.stack(parts), EP, 0, 0)  25.5 us
  transfers between devices with their start and end apart: 9, of which 6 were waited for; matrix products, arithmetic and copies ran while one was open for 36% of the time, Pallas kernels for 0%

profile of v1, /device:TPU:33, one launch (start us, length us, event | category | flops | bytes accessed | tf_op | source)
XLA Modules:
  0.0 596.4 jit_solution(535935145309427397)
XLA Ops:
  38.0 25.5 %all-to-all-start.3 = ((bf16[32,1,12,2048]{3,2,1,0:T(8,128)(2,1)}), bf16[32,1,12,2048]{3,2,1,0:T(8,128)(2,1)}, u32[]{:S(2)}, u32[]{:S(2)}) async-start(bf16[32,1,12,2048]{3,2,1,0:T(8,128)(2,1)} %fusion.41), calls=%async_computation.3 | async-start | bytes 4194304 | tf_op jit(solution)/shard_map/all_to_all | solution.py:221
  63.6 45.3 %all-gather.8.cloned.1.call-done = bf16[6144,128]{0,1:T(8,128)(2,1)} async-done(((bf16[384,128]{0,1:T(8,128)(2,1)}), bf16[6144,128]{0,1:T(8,128)(2,1)}) %all-gather.8.cloned.1.call-update) | async-done | bytes 1572880 | tf_op jit(solution)/shard_map/all_gather | solution.py:24
  111.6 55.8 %all-to-all-done.3 = bf16[32,1,12,2048]{3,2,1,0:T(8,128)(2,1)} async-done(((bf16[32,1,12,2048]{3,2,1,0:T(8,128)(2,1)}), bf16[32,1,12,2048]{3,2,1,0:T(8,128)(2,1)}, u32[]{:S(2)}, u32[]{:S(2)}) %all-to-all-start.3) | async-done | bytes 1572896 | tf_op jit(solution)/shard_map/all_to_all | solution.py:221
  172.8 4.7 all-to-all-start.1
  179.5 37.5 %all-to-all-done.1 = bf16[4,128,2048]{2,1,0:T(8,128)(2,1)} async-done(((bf16[4,128,2048]{2,1,0:T(8,128)(2,1)}), bf16[4,128,2048]{2,1,0:T(8,128)(2,1)}, u32[]{:S(2)}, u32[]{:S(2)}) %all-to-all-start.1) | async-done | bytes 2097184 | tf_op jit(solution)/shard_map/all_to_all | solution.py:37
  219.4 5.5 convolution_convert_fusion
  224.9 4.8 all-to-all-start.2
  233.6 43.9 %all-gather.6.cloned.1.call-done = bf16[4,32,2,6,2048]{4,1,3,0,2:T(8,128)(2,1)} async-done(((bf16[1,32,2,6,2048]{4,1,3,0,2:T(8,128)(2,1)}), bf16[4,32,2,6,2048]{4,1,3,0,2:T(8,128)(2,1)}) %all-gather.6.cloned.1.call-update) | async-done | bytes 6291472 | tf_op jit(solution)/shard_map/all_gather | solution.py:225
  277.6 6.4 %fusion.14 = f32[2,4,32,6,256]{4,2,3,1,0:T(8,128)} fusion(bf16[4,32,2,6,2048]{4,1,3,0,2:T(8,128)(2,1)} %all-gather.6.cloned.1.call-done, bf16[2,2048,256]{2,1,0:T(8,128)(2,1)} %param.28), kind=kOutput, calls=%fused_computation.27 | convolution fusion | flops 1610612736 | bytes 9961472 | tf_op jit(solution)/shard_map/osjcd,jdf->osjcf/dot_general | solution.py:145
  284.0 10.1 %convert_bitcast_fusion = bf16[4,32,2,6,2048]{4,1,3,0,2:T(8,128)(2,1)} fusion(bf16[2,256,2048]{2,1,0:T(8,128)(2,1)S(1)} %copy-done, f32[2,4,32,6,256]{4,2,3,1,0:T(8,128)} %fusion.14, bf16[4,32,2,6,2048]{4,1,3,0,2:T(8,128)(2,1)} %all-gather.6.cloned.1.call-done, bf16[2,2048,256]{2,1,0:T(8,128)(2,1)} %param.29), kind=kOutput, calls=%fused_computation.20 | convolution fusion | flops 3226730496 | bytes 18350080 | tf_op jit(solution)/shard_map/osjcf,jfd->osjcd/dot_general | solution.py:227
  294.1 10.2 %copy.98 = bf16[4,32,2,6,2048]{4,0,3,2,1:T(4,128)(2,1)} copy(bf16[4,32,2,6,2048]{4,1,3,0,2:T(8,128)(2,1)} %convert_bitcast_fusion) | data formatting | bytes 12582912 | tf_op jit(solution)/shard_map/convert_element_type | solution.py:234
  304.3 9.1 %copy.99 = bf16[4,384,2048]{2,1,0:T(8,128)(2,1)} copy(bf16[4,384,2048]{2,0,1:T(4,128)(2,1)} %bitcast.275) | data formatting | bytes 12582912 | tf_op jit(solution)/shard_map/convert_element_type | solution.py:234
  313.4 5.3 all-to-all-start.4
  318.7 127.6 %while.15 = (s32[]{:T(128)}, f32[4,384]{1,0:T(4,128)S(1)}, f32[4,384]{1,0:T(4,128)S(1)}, f32[4,384,64]{1,2,0:T(8,128)S(1)}, bf16[12,1024,128]{2,1,0:T(8,128)(2,1...) while((s32[]{:T(128)}, f32[4,384]{1,0:T(4,128)S(1)}, f32[4,384]{1,0:T(4,128)S(1)}, ...), condition=%wide.region_5.6_spmd.clone, body=%wide.region_2.5_spmd.clone.sunk | while | flops 415538688 | bytes 46432384 | solution.py:134
  334.2 4.0 fusion.108
  344.8 4.0 fusion.108
  376.7 4.0 fusion.108
  408.6 4.0 fusion.108
  448.2 4.1 all-to-all-start
  452.3 5.7 reduce_sum.96
  461.6 10.4 %all-to-all-done = bf16[4,96,2048]{2,1,0:T(8,128)(2,1)S(1)} async-done(((bf16[4,96,2048]{2,1,0:T(8,128)(2,1)}), bf16[4,96,2048]{2,1,0:T(8,128)(2,1)S(1)}, u32[]{:S(2)}, u32[]{:S(2)}) %all-to-all-start) | async-done | bytes 1572896 | tf_op jit(solution)/shard_map/all_to_all | solution.py:52
  472.0 8.5 %all-to-all-start.5 = ((bf16[32,12,2048]{2,1,0:T(8,128)(2,1)}), bf16[32,12,2048]{2,1,0:T(8,128)(2,1)}, u32[]{:S(2)}, u32[]{:S(2)}) async-start(bf16[32,12,2048]{2,1,0:T(8,128)(2,1)} %all_to_all.28), calls=%async_computation.5 | async-start | bytes 4194304 | tf_op jit(solution)/shard_map/all_to_all | solution.py:237
  484.0 95.3 %all-to-all-done.5 = bf16[32,12,2048]{2,1,0:T(8,128)(2,1)} async-done(((bf16[32,12,2048]{2,1,0:T(8,128)(2,1)}), bf16[32,12,2048]{2,1,0:T(8,128)(2,1)}, u32[]{:S(2)}, u32[]{:S(2)}) %all-to-all-start.5) | async-done | bytes 1572896 | tf_op jit(solution)/shard_map/all_to_all | solution.py:237
  583.5 4.0 gather_fusion.2
  (245 shorter events, 173.7 us)
Async XLA Ops:
  7.2 276.8 %copy-start = (bf16[2,256,2048]{2,1,0:T(8,128)(2,1)S(1)}, bf16[2,256,2048]{2,1,0:T(8,128)(2,1)}, u32[]{:S(2)}) copy-start(bf16[2,256,2048]{2,1,0:T(8,128)(2,1)} %param.30) | copy-start | bytes 6291460
  7.2 5.3 copy-start.4
  7.2 5.5 copy-start.7
  7.2 101.6 %all-gather.8.cloned.1.call-start = ((), (), s32[]{:S(2)}) async-start(), calls=%async_computation.7 | async-start | bytes 1671168 | tf_op jit(solution)/shard_map/all_gather | solution.py:24
  38.0 129.4 %all-to-all-start.3 = ((bf16[32,1,12,2048]{3,2,1,0:T(8,128)(2,1)}), bf16[32,1,12,2048]{3,2,1,0:T(8,128)(2,1)}, u32[]{:S(2)}, u32[]{:S(2)}) async-start(bf16[32,1,12,2048]{3,2,1,0:T(8,128)(2,1)} %fusion.41), calls=%async_computation.3 | async-start | bytes 4194304 | tf_op jit(solution)/shard_map/all_to_all | solution.py:221
  63.5 166.2 %all-gather.10.cloned.1.call-start = ((), (), s32[]{:S(2)}) async-start(), calls=%async_computation.8 | async-start | bytes 4718592 | tf_op jit(solution)/shard_map/all_gather | solution.py:24
  111.5 166.0 %all-gather.6.cloned.1.call-start = ((), (), s32[]{:S(2)}) async-start(), calls=%async_computation.6 | async-start | bytes 7864320 | tf_op jit(solution)/shard_map/all_gather | solution.py:225
  172.8 4.7 copy-start.6
  172.8 5.1 copy-start.10
  172.8 44.2 %all-to-all-start.1 = ((bf16[4,128,2048]{2,1,0:T(8,128)(2,1)}), bf16[4,128,2048]{2,1,0:T(8,128)(2,1)}, u32[]{:S(2)}, u32[]{:S(2)}) async-start(bf16[4,128,2048]{2,1,0:T(8,128)(2,1)} %broadcast_in_dim.47), calls=%async_computation.1 | async-start | bytes 4194304 | tf_op jit(solution)/shard_map/all_to_all | solution.py:37
  224.9 88.5 %all-to-all-start.2 = ((bf16[4,128,2048]{2,1,0:T(8,128)(2,1)}), bf16[4,128,2048]{2,1,0:T(8,128)(2,1)}, u32[]{:S(2)}, u32[]{:S(2)}) async-start(bf16[4,128,2048]{2,1,0:T(8,128)(2,1)} %bitcast.276), calls=%async_computation.2 | async-start | bytes 4194304 | tf_op jit(solution)/shard_map/all_to_all | solution.py:52
  313.4 134.8 %all-to-all-start.4 = ((bf16[4,384,2048]{2,1,0:T(8,128)(2,1)}), bf16[4,384,2048]{2,1,0:T(8,128)(2,1)}, u32[]{:S(2)}, u32[]{:S(2)}) async-start(bf16[4,384,2048]{2,1,0:T(8,128)(2,1)} %copy.99), calls=%async_computation.4 | async-start | bytes 12582912 | tf_op jit(solution)/shard_map/all_to_all | solution.py:52
  318.7 127.7 %copy-start.5 = (bf16[256,2048]{1,0:T(8,128)(2,1)S(1)}, bf16[256,2048]{1,0:T(8,128)(2,1)}, u32[]{:S(2)}) copy-start(bf16[256,2048]{1,0:T(8,128)(2,1)} %param.23) | copy-start | bytes 3145732
  323.5 4.6 copy-start.2
  334.2 4.6 copy-start.2
  344.8 4.6 copy-start.2
  366.0 4.6 copy-start.2
  376.7 4.6 copy-start.2
  397.9 4.6 copy-start.2
  429.8 4.6 copy-start.2
  448.2 23.8 %all-to-all-start = ((bf16[4,96,2048]{2,1,0:T(8,128)(2,1)}), bf16[4,96,2048]{2,1,0:T(8,128)(2,1)S(1)}, u32[]{:S(2)}, u32[]{:S(2)}) async-start(bf16[4,96,2048]{2,1,0:T(8,128)(2,1)} %bitcast.280), calls=%async_computation | async-start | bytes 3145728 | tf_op jit(solution)/shard_map/all_to_all | solution.py:52
  461.6 19.2 %copy-start.9 = (f32[128,2]{0,1:T(2,128)S(1)}, f32[128,2]{0,1:T(2,128)}, u32[]{:S(2)}) copy-start(f32[128,2]{0,1:T(2,128)} %param.27) | copy-start | bytes 3076
  472.0 107.2 %all-to-all-start.5 = ((bf16[32,12,2048]{2,1,0:T(8,128)(2,1)}), bf16[32,12,2048]{2,1,0:T(8,128)(2,1)}, u32[]{:S(2)}, u32[]{:S(2)}) async-start(bf16[32,12,2048]{2,1,0:T(8,128)(2,1)} %all_to_all.28), calls=%async_computation.5 | async-start | bytes 4194304 | tf_op jit(solution)/shard_map/all_to_all | solution.py:237
  583.5 6.4 %copy-start.1 = (bf16[2,256,2048]{2,1,0:T(8,128)(2,1)S(1)}, bf16[2,256,2048]{2,1,0:T(8,128)(2,1)}, u32[]{:S(2)}) copy-start(bf16[2,256,2048]{2,1,0:T(8,128)(2,1)} %param.30) | copy-start | bytes 6291460
  (7 other events, 28.3 us)
Sparse Core Ops, SparseCore 0:
  10.9 97.9 all-gather.7
  111.6 33.0 all-gather.9
  171.2 106.2 all-gather.5
